TPU v7x, 256 devices: a whole 4x4x8 slice. The times are simulated.
256 devices in a mesh: kv: 16 (over y, x), tp: 16 (over z, core).
Axes of the slice: x: 4, y: 4, z: 8, core: 2. Of those that a mesh axis runs over, the one named last changes fastest.
Arguments:
- tokens: bfloat16 [256, 4096], P(None, ('kv', 'tp')), may hold values from -6 to 6
- memory: float32 [256, 16, 256, 128], P('kv', 'tp'), may hold values from -6 to 6
- normalizer: float32 [256, 16, 128], P('kv', 'tp'), may hold values from -6 to 6
- stabilizer: float32 [256, 16], P('kv', 'tp'), may hold values from -4 to 4
- first_gain: float32 [4096], replicated, may hold values from 0.1 to 1.9
- first_gate: bfloat16 [4096, 12288], P('kv', 'tp'), may hold values from -0.09375 to 0.09375
- first_up: bfloat16 [4096, 12288], P('kv', 'tp'), may hold values from -0.09375 to 0.09375
- first_down: bfloat16 [12288, 4096], P('tp', 'kv'), may hold values from -0.078125 to 0.078125
- mixer_gain: float32 [4096], replicated, may hold values from 0.1 to 1.9
- query_weight: bfloat16 [4096, 2048], P(None, 'tp'), may hold values from -0.09375 to 0.09375
- key_weight: bfloat16 [4096, 2048], P(None, 'tp'), may hold values from -0.09375 to 0.09375
- value_weight: bfloat16 [4096, 4096], P(None, 'tp'), may hold values from -0.09375 to 0.09375
- input_weight: bfloat16 [4096, 16], replicated, may hold values from -0.09375 to 0.09375
- forget_weight: bfloat16 [4096, 16], replicated, may hold values from -0.09375 to 0.09375
- forget_bias: float32 [16], P('tp'), may hold values from -2 to 4
- output_weight: bfloat16 [4096, 4096], P('tp'), may hold values from -0.09375 to 0.09375
- last_gain: float32 [4096], replicated, may hold values from 0.1 to 1.9
- last_gate: bfloat16 [4096, 12288], P('kv', 'tp'), may hold values from -0.09375 to 0.09375
- last_up: bfloat16 [4096, 12288], P('kv', 'tp'), may hold values from -0.09375 to 0.09375
- last_down: bfloat16 [12288, 4096], P('tp', 'kv'), may hold values from -0.078125 to 0.078125
Outputs:
- result: bfloat16 [256, 4096], P(None, ('kv', 'tp'))
- new_memory: float32 [256, 16, 256, 128], P('kv', 'tp')
- new_normalizer: float32 [256, 16, 128], P('kv', 'tp')
- new_stabilizer: float32 [256, 16], P('kv', 'tp')
All inputs are finite; a program needn't handle non-finite values.
Results may differ from a plain program's by a relative error of at most 0.025.
Values may be sent and summed in bfloat16 or wider, within the bound.
A program may use at most 64 MiB of HBM per device.

v0:
```python
import math

import jax
import jax.numpy as jnp
from jax import lax
from jax.sharding import PartitionSpec as P

EPS = 1e-06


def in_blocks(array, dim, size):
    before, after = (array.shape[:dim], array.shape[dim + 1 :])
    return jnp.moveaxis(array.reshape(*before, size, -1, *after), dim, 0)


def summed_on_arrival(array, axis, dim):
    size = lax.axis_size(axis)
    tiles = lax.all_to_all(in_blocks(array, dim, size), axis, 0, 0, tiled=True)
    return jnp.sum(tiles.astype(jnp.float32), axis=0)


def side_by_side(arrays, axis, dim, along):
    widths = [math.prod(a.shape[along:]) for a in arrays]
    both = jnp.concatenate(
        [a.reshape(*a.shape[:along], w) for a, w in zip(arrays, widths)], axis=along
    )
    out = summed_on_arrival(both, axis, dim)
    tiles = jnp.split(out, [sum(widths[:k]) for k in range(1, len(widths))], axis=along)
    return tuple((b.reshape(*out.shape[:along], *a.shape[along:]) for a, b in zip(arrays, tiles)))


def in_order(tiles, dim):
    tiles = jnp.moveaxis(tiles, 0, dim)
    shape = tiles.shape
    return tiles.reshape(*shape[:dim], shape[dim] * shape[dim + 1], *shape[dim + 2 :])


def from_everyone(array, axis):
    copies = jnp.broadcast_to(array, (lax.axis_size(axis), *array.shape))
    return lax.all_to_all(copies, axis, split_axis=0, concat_axis=0, tiled=True)


def collect(array, axis, dim):
    return in_order(from_everyone(array, axis), dim)


def total_of_pieces(array, axis):
    tiles = lax.all_gather(array, axis).astype(jnp.float32)
    return tiles.sum(axis=0)


def hidden_units(gate_acc, up_acc, squares, model_width):
    scale = lax.rsqrt(squares / model_width + EPS)[:, None]
    return (jax.nn.silu(scale * gate_acc) * (scale * up_acc)).astype(jnp.bfloat16)


def gated_block(block, gain, w_gate, w_up, w_down, model_width):
    f32 = jnp.float32
    width = block.shape[1]
    gain_block = lax.dynamic_slice_in_dim(gain, lax.axis_index("kv") * width, width, 0)
    values = block.astype(f32)
    scaled = (values * gain_block).astype(jnp.bfloat16)
    gate_part = jnp.dot(scaled, w_gate, preferred_element_type=f32)
    up_part = jnp.dot(scaled, w_up, preferred_element_type=f32)
    squares = jnp.sum(values * values, axis=1)
    gate_acc, up_acc, sq_total = side_by_side(
        (
            gate_part.astype(jnp.bfloat16),
            up_part.astype(jnp.bfloat16),
            squares.astype(jnp.bfloat16),
        ),
        "kv",
        0,
        1,
    )
    hidden_share = hidden_units(gate_acc, up_acc, sq_total, model_width)
    partial_value = lax.dot_general(
        w_down, collect(hidden_share, "kv", 0), (((0,), (1,)), ((), ())), preferred_element_type=f32
    )
    share = summed_on_arrival(partial_value.astype(jnp.bfloat16), "tp", 0)
    return share.T


def body(
    tokens,
    memory,
    normalizer,
    stabilizer,
    first_gain,
    first_gate,
    first_up,
    first_down,
    mixer_gain,
    query_weight,
    key_weight,
    value_weight,
    input_weight,
    forget_weight,
    forget_bias,
    output_weight,
    last_gain,
    last_gate,
    last_up,
    last_down,
):
    f32 = jnp.float32
    model_width = first_gain.shape[0]
    rows, col_width = tokens.shape
    block = collect(tokens, "tp", 1)
    first_share = gated_block(block, first_gain, first_gate, first_up, first_down, model_width)
    stream_one = (tokens.astype(f32) + 0.5 * first_share).astype(jnp.bfloat16)
    seq_count, head_count, value_size, key_size = memory.shape
    moved = lax.all_to_all(
        stream_one.reshape(rows, 1, col_width), "kv", split_axis=0, concat_axis=1, tiled=True
    )
    own_rows = collect(moved, "tp", 2).reshape(seq_count, model_width)
    row_values = own_rows.astype(f32)
    scale = lax.rsqrt(jnp.mean(row_values * row_values, axis=1, keepdims=True) + EPS)
    cell_in = (row_values * mixer_gain).astype(jnp.bfloat16)
    query = (
        scale * jnp.dot(cell_in, query_weight, preferred_element_type=f32) * key_size ** (-0.5)
    ).reshape(seq_count, head_count, key_size)
    key = (scale * jnp.dot(cell_in, key_weight, preferred_element_type=f32)).reshape(
        seq_count, head_count, key_size
    )
    value = (scale * jnp.dot(cell_in, value_weight, preferred_element_type=f32)).reshape(
        seq_count, head_count, value_size
    )
    first_head = lax.axis_index("tp") * head_count
    input_all = scale * jnp.dot(cell_in, input_weight, preferred_element_type=f32)
    forget_all = scale * jnp.dot(cell_in, forget_weight, preferred_element_type=f32)
    input_pre = lax.dynamic_slice_in_dim(input_all, first_head, head_count, 1)
    log_forget = jax.nn.log_sigmoid(
        lax.dynamic_slice_in_dim(forget_all, first_head, head_count, 1) + forget_bias
    )
    carried = log_forget + stabilizer
    new_stabilizer = jnp.maximum(carried, input_pre)
    keep = jnp.exp(carried - new_stabilizer)
    admit = jnp.exp(input_pre - new_stabilizer)
    recalled = jnp.einsum("bhvd,bhd->bhv", memory, query, precision=lax.Precision.HIGHEST)
    match = jnp.sum(query * key, axis=-1)
    numer = keep[..., None] * recalled + (admit * match)[..., None] * value
    denom = keep * jnp.sum(normalizer * query, axis=-1) + admit * match
    cell_out = (
        (numer / jnp.maximum(jnp.abs(denom), 1.0)[..., None])
        .reshape(seq_count, head_count * value_size)
        .astype(jnp.bfloat16)
    )
    new_memory = (
        keep[..., None, None] * memory
        + admit[..., None, None] * value[..., :, None] * key[..., None, :]
    )
    new_normalizer = keep[..., None] * normalizer + admit[..., None] * key
    partial_heads = jnp.dot(cell_out, output_weight, preferred_element_type=f32)
    mixed = total_of_pieces(partial_heads.astype(jnp.bfloat16), "tp").astype(jnp.float32)
    rows_two = (row_values + mixed).astype(jnp.bfloat16)
    whole_two = lax.all_to_all(rows_two, "kv", split_axis=1, concat_axis=0, tiled=True)
    last_share = gated_block(whole_two, last_gain, last_gate, last_up, last_down, model_width)
    own_columns = lax.dynamic_slice_in_dim(
        whole_two, lax.axis_index("tp") * col_width, col_width, 1
    )
    result = (own_columns.astype(f32) + 0.5 * last_share).astype(jnp.bfloat16)
    return (result, new_memory, new_normalizer, new_stabilizer)


def solution(mesh):
    in_specs = (
        P(None, ("kv", "tp")),
        P("kv", "tp", None, None),
        P("kv", "tp", None),
        P("kv", "tp"),
        P(),
        P("kv", "tp"),
        P("kv", "tp"),
        P("tp", "kv"),
        P(),
        P(None, "tp"),
        P(None, "tp"),
        P(None, "tp"),
        P(),
        P(),
        P("tp"),
        P("tp", None),
        P(),
        P("kv", "tp"),
        P("kv", "tp"),
        P("tp", "kv"),
    )
    out_specs = (
        P(None, ("kv", "tp")),
        P("kv", "tp", None, None),
        P("kv", "tp", None),
        P("kv", "tp"),
    )
    return jax.shard_map(body, mesh=mesh, in_specs=in_specs, out_specs=out_specs, check_vma=False)
```

profile of v0, /device:TPU:1, one launch (start us, length us, event | category | flops | bytes accessed | tf_op | source)
XLA Modules:
  0.0 225.0 jit_solution(10752747142015780594)
XLA Ops:
  7.2 1.5 broadcast_in_dim.8
  8.7 10.0 %all-to-all-start = ((bf16[16,256,16]{1,2,0:T(8,128)(2,1)}), bf16[16,256,16]{1,2,0:T(8,128)(2,1)S(1)}, u32[]{:S(2)}, u32[]{:S(2)}) async-start(bf16[16,256,16]{1,2,0:T(8,128)(2,1)} %broadcast_in_dim.8), calls=%async_computation | async-start | bytes 262144 | tf_op jit(solution)/shard_map/all_to_all | solution.py:40
  19.4 8.1 %all-to-all-done = bf16[16,256,16]{1,2,0:T(8,128)(2,1)S(1)} async-done(((bf16[16,256,16]{1,2,0:T(8,128)(2,1)}), bf16[16,256,16]{1,2,0:T(8,128)(2,1)S(1)}, u32[]{:S(2)}, u32[]{:S(2)}) %all-to-all-start) | async-done | bytes 131104 | tf_op jit(solution)/shard_map/all_to_all | solution.py:40
  28.0 1.3 convolution_convert_fusion.3
  29.3 1.3 convolution_convert_fusion.4
  30.6 21.4 %all_to_all.74 = bf16[16,16,1537]{2,1,0:T(8,128)(2,1)S(1)} all-to-all(bf16[16,16,1537]{2,1,0:T(8,128)(2,1)S(1)} %pad_maximum_fusion), channel_id=1, replica_groups=mesh['kv'=16,'tp'=16] {'kv'}, dimensions={0} | all-to-all | bytes 1573888 | tf_op jit(solution)/shard_map/all_to_all | solution.py:18
  52.4 12.0 %all_to_all.75 = bf16[16,16,768]{2,1,0:T(8,128)(2,1)S(1)} all-to-all(bf16[16,16,768]{2,1,0:T(8,128)(2,1)S(1)} %broadcast_in_dim.9), channel_id=1, replica_groups=mesh['kv'=16,'tp'=16] {'kv'}, dimensions={0} | all-to-all | bytes 786432 | tf_op jit(solution)/shard_map/all_to_all | solution.py:40
  64.7 13.6 %all_to_all.76 = bf16[16,16,256]{2,1,0:T(8,128)(2,1)S(1)} all-to-all(bf16[16,16,256]{2,1,0:T(8,128)(2,1)S(1)} %bitcast.135), channel_id=1, replica_groups=mesh['kv'=16,'tp'=16] {'tp'}, dimensions={0} | all-to-all | bytes 262144 | tf_op jit(solution)/shard_map/all_to_all | solution.py:18
  79.8 9.1 %all_to_all.77 = bf16[16,2,128]{2,1,0:T(2,128)(2,1)S(1)} all-to-all(bf16[16,2,128]{2,1,0:T(2,128)(2,1)S(1)} %reshape.151), channel_id=1, replica_groups=mesh['kv'=16,'tp'=16] {'kv'}, dimensions={0} | all-to-all | bytes 16384 | tf_op jit(solution)/shard_map/all_to_all | solution.py:113
  89.5 1.8 reshape.153
  91.3 4.4 %all-to-all-start.5 = ((bf16[16,2,2048]{2,1,0:T(2,128)(2,1)}), bf16[16,2,2048]{2,1,0:T(2,128)(2,1)S(1)}, u32[]{:S(2)}, u32[]{:S(2)}) async-start(bf16[16,2,2048]{2,1,0:T(2,128)(2,1)} %reshape.153), calls=%async_computation.5 | async-start | bytes 262144 | tf_op jit(solution)/shard_map/all_to_all | solution.py:40
  96.5 8.3 %all-to-all-done.5 = bf16[16,2,2048]{2,1,0:T(2,128)(2,1)S(1)} async-done(((bf16[16,2,2048]{2,1,0:T(2,128)(2,1)}), bf16[16,2,2048]{2,1,0:T(2,128)(2,1)S(1)}, u32[]{:S(2)}, u32[]{:S(2)}) %all-to-all-start.5) | async-done | bytes 131104 | tf_op jit(solution)/shard_map/all_to_all | solution.py:40
  106.2 2.5 %copy.58 = f32[16,16,16,16]{3,2,1,0:T(8,128)} copy(f32[16,16,16,16]{3,1,0,2:T(8,128)S(1)} %convert_bitcast_fusion) | data formatting | bytes 524288 | tf_op jit(solution)/shard_map/convert_element_type | solution.py:117
  108.7 3.2 %reshape.144 = f32[16,4096]{1,0:T(8,128)S(1)} reshape(f32[16,16,16,16]{3,2,1,0:T(8,128)} %copy.58) | data formatting | bytes 524288 | tf_op jit(solution)/shard_map/convert_element_type | solution.py:117
  112.0 0.9 multiply_convert_fusion.1
  113.0 1.1 fusion.39
  114.4 1.7 multiply_reduce_fusion.2
  116.6 0.8 bitcast_add_fusion.3
  117.4 1.8 fusion.1
  119.3 1.1 convolution_convert_fusion
  120.4 2.4 %reshape.143 = f32[16,16,256]{2,1,0:T(8,128)S(1)} reshape(f32[16,16,16,16]{3,2,1,0:T(8,128)} %copy.58) | data formatting | bytes 524288 | tf_op jit(solution)/shard_map/convert_element_type | solution.py:117
  122.9 30.1 %all-gather.3.cloned.1.call-done = bf16[256,4096]{1,0:T(8,128)(2,1)} async-done(((bf16[16,4096]{1,0:T(8,128)(2,1)}), bf16[256,4096]{1,0:T(8,128)(2,1)}) %all-gather.3.cloned.1.call-update) | async-done | bytes 2097168 | tf_op jit(solution)/shard_map/all_gather | solution.py:48
  153.0 2.0 convert_reduce_fusion
  155.8 6.5 %all-to-all-start.6 = ((bf16[16,16,256]{2,0,1:T(8,128)(2,1)}), bf16[16,16,256]{2,0,1:T(8,128)(2,1)S(1)}, u32[]{:S(2)}, u32[]{:S(2)}) async-start(bf16[16,16,256]{2,0,1:T(8,128)(2,1)} %copy.61), calls=%async_computation.6 | async-start | bytes 262144 | tf_op jit(solution)/shard_map/all_to_all | solution.py:157
  163.1 6.1 %all-to-all-done.6 = bf16[16,16,256]{2,0,1:T(8,128)(2,1)S(1)} async-done(((bf16[16,16,256]{2,0,1:T(8,128)(2,1)}), bf16[16,16,256]{2,0,1:T(8,128)(2,1)S(1)}, u32[]{:S(2)}, u32[]{:S(2)}) %all-to-all-start.6) | async-done | bytes 131104 | tf_op jit(solution)/shard_map/all_to_all | solution.py:157
  170.3 16.5 %all_to_all.78 = bf16[16,16,1537]{2,1,0:T(8,128)(2,1)S(1)} all-to-all(bf16[16,16,1537]{2,1,0:T(8,128)(2,1)S(1)} %pad_maximum_fusion.1), channel_id=1, replica_groups=mesh['kv'=16,'tp'=16] {'kv'}, dimensions={0} | all-to-all | bytes 1573888 | tf_op jit(solution)/shard_map/all_to_all | solution.py:18
  187.9 3.6 %all-to-all-start.8 = ((bf16[16,16,768]{2,1,0:T(8,128)(2,1)}), bf16[16,16,768]{2,1,0:T(8,128)(2,1)S(1)}, u32[]{:S(2)}, u32[]{:S(2)}) async-start(bf16[16,16,768]{2,1,0:T(8,128)(2,1)} %broadcast_in_dim.11), calls=%async_computation.8 | async-start | bytes 786432 | tf_op jit(solution)/shard_map/all_to_all | solution.py:40
  191.5 8.2 %all-to-all-done.8 = bf16[16,16,768]{2,1,0:T(8,128)(2,1)S(1)} async-done(((bf16[16,16,768]{2,1,0:T(8,128)(2,1)}), bf16[16,16,768]{2,1,0:T(8,128)(2,1)S(1)}, u32[]{:S(2)}, u32[]{:S(2)}) %all-to-all-start.8) | async-done | bytes 393248 | tf_op jit(solution)/shard_map/all_to_all | solution.py:40
  199.7 1.0 convolution_convert_fusion.5
  200.7 8.0 %all-to-all-start.9 = ((bf16[16,16,256]{2,1,0:T(8,128)(2,1)}), bf16[16,16,256]{2,1,0:T(8,128)(2,1)S(1)}, u32[]{:S(2)}, u32[]{:S(2)}) async-start(bf16[16,16,256]{2,1,0:T(8,128)(2,1)} %bitcast.33), calls=%async_computation.9 | async-start | bytes 262144 | tf_op jit(solution)/shard_map/all_to_all | solution.py:18
  208.6 2.9 %multiply_add_fusion = f32[16,1,256,128]{3,2,1,0:T(8,128)} fusion(f32[16,1,256,128]{3,2,1,0:T(8,128)} %param.21, f32[16,128]{1,0:T(8,128)S(1)} %convolution_multiply_fusion.1, f32[16,256]{1,0:T(8,128)S(1)} %get-tuple-element.29, f32[16]{0:T(128)S(1)} %get-tuple-element.20), kind=kLoop, calls=%fused_computation.7 | loop fusion | flops 1572864 | bytes 4218944 | tf_op jit(solution)/shard_map/add | solution.py:150
  211.7 5.8 %all-to-all-done.9 = bf16[16,16,256]{2,1,0:T(8,128)(2,1)S(1)} async-done(((bf16[16,16,256]{2,1,0:T(8,128)(2,1)}), bf16[16,16,256]{2,1,0:T(8,128)(2,1)S(1)}, u32[]{:S(2)}, u32[]{:S(2)}) %all-to-all-start.9) | async-done | bytes 131104 | tf_op jit(solution)/shard_map/all_to_all | solution.py:18
  (77 shorter events, 10.9 us)
Async XLA Ops:
  7.2 112.1 %copy-start = (bf16[256,4096]{1,0:T(8,128)(2,1)S(1)}, bf16[256,4096]{1,0:T(8,128)(2,1)}, u32[]{:S(2)}) copy-start(bf16[256,4096]{1,0:T(8,128)(2,1)} %param.35) | copy-start | bytes 6291460
  8.7 18.9 %all-to-all-start = ((bf16[16,256,16]{1,2,0:T(8,128)(2,1)}), bf16[16,256,16]{1,2,0:T(8,128)(2,1)S(1)}, u32[]{:S(2)}, u32[]{:S(2)}) async-start(bf16[16,256,16]{1,2,0:T(8,128)(2,1)} %broadcast_in_dim.8), calls=%async_computation | async-start | bytes 262144 | tf_op jit(solution)/shard_map/all_to_all | solution.py:40
  30.6 33.8 %copy-start.4 = (bf16[768,256]{1,0:T(8,128)(2,1)S(1)}, bf16[768,256]{1,0:T(8,128)(2,1)}, u32[]{:S(2)}) copy-start(bf16[768,256]{1,0:T(8,128)(2,1)} %param.27) | copy-start | bytes 1179652
  52.0 26.3 %copy-start.9 = (bf16[256,16]{0,1:T(8,128)(2,1)S(1)}, bf16[256,16]{0,1:T(8,128)(2,1)}, u32[]{:S(2)}) copy-start(bf16[256,16]{0,1:T(8,128)(2,1)} %param.20) | copy-start | bytes 24580
  91.3 13.6 %all-to-all-start.5 = ((bf16[16,2,2048]{2,1,0:T(2,128)(2,1)}), bf16[16,2,2048]{2,1,0:T(2,128)(2,1)S(1)}, u32[]{:S(2)}, u32[]{:S(2)}) async-start(bf16[16,2,2048]{2,1,0:T(2,128)(2,1)} %reshape.153), calls=%async_computation.5 | async-start | bytes 262144 | tf_op jit(solution)/shard_map/all_to_all | solution.py:40
  95.7 57.3 %all-gather.3.cloned.1.call-start = ((), (), s32[]{:S(2)}) async-start(), calls=%async_computation.10 | async-start | bytes 2228224 | tf_op jit(solution)/shard_map/all_gather | solution.py:48
  108.7 4.1 %copy-start.8 = (bf16[4096,16]{0,1:T(8,128)(2,1)S(1)}, bf16[4096,16]{0,1:T(8,128)(2,1)}, u32[]{:S(2)}) copy-start(bf16[4096,16]{0,1:T(8,128)(2,1)} %param.32) | copy-start | bytes 393220
  108.7 5.4 %copy-start.3 = (bf16[4096,128]{1,0:T(8,128)(2,1)S(1)}, bf16[4096,128]{1,0:T(8,128)(2,1)}, u32[]{:S(2)}) copy-start(bf16[4096,128]{1,0:T(8,128)(2,1)} %param.30) | copy-start | bytes 3145732
  112.0 4.2 %copy-start.12 = (f32[16,1]{0,1:T(1,128)S(1)}, f32[16,1]{0,1:T(1,128)}, u32[]{:S(2)}) copy-start(f32[16,1]{0,1:T(1,128)} %param.23) | copy-start | bytes 196
  112.0 4.3 %copy-start.2 = (bf16[4096,256]{1,0:T(8,128)(2,1)S(1)}, bf16[4096,256]{1,0:T(8,128)(2,1)}, u32[]{:S(2)}) copy-start(bf16[4096,256]{1,0:T(8,128)(2,1)} %param.31) | copy-start | bytes 6291460
  114.1 2.5 %copy-start.10 = (f32[16,1,128]{2,1,0:T(1,128)S(1)}, f32[16,1,128]{2,1,0:T(1,128)}, u32[]{:S(2)}) copy-start(f32[16,1,128]{2,1,0:T(1,128)} %param.22) | copy-start | bytes 24580
  114.1 3.3 %copy-start.1 = (f32[16,1,256,128]{3,2,1,0:T(8,128)S(1)}, f32[16,1,256,128]{3,2,1,0:T(8,128)}, u32[]{:S(2)}) copy-start(f32[16,1,256,128]{3,2,1,0:T(8,128)} %param.21) | copy-start | bytes 6291460
  116.2 3.1 %copy-start.11 = (f32[16,1]{0,1:T(1,128)}, f32[16,1]{0,1:T(1,128)S(1)}, u32[]{:S(2)}) copy-start(f32[16,1]{0,1:T(1,128)S(1)} %get-tuple-element.21) | copy-start | bytes 196
  153.0 16.6 %copy-start.6 = (bf16[256,768]{1,0:T(8,128)(2,1)S(1)}, bf16[256,768]{1,0:T(8,128)(2,1)}, u32[]{:S(2)}) copy-start(bf16[256,768]{1,0:T(8,128)(2,1)} %param.38) | copy-start | bytes 1179652
  153.0 16.9 %copy-start.7 = (bf16[256,768]{1,0:T(8,128)(2,1)S(1)}, bf16[256,768]{1,0:T(8,128)(2,1)}, u32[]{:S(2)}) copy-start(bf16[256,768]{1,0:T(8,128)(2,1)} %param.37) | copy-start | bytes 1179652
  155.8 13.4 %all-to-all-start.6 = ((bf16[16,16,256]{2,0,1:T(8,128)(2,1)}), bf16[16,16,256]{2,0,1:T(8,128)(2,1)S(1)}, u32[]{:S(2)}, u32[]{:S(2)}) async-start(bf16[16,16,256]{2,0,1:T(8,128)(2,1)} %copy.61), calls=%async_computation.6 | async-start | bytes 262144 | tf_op jit(solution)/shard_map/all_to_all | solution.py:157
  170.3 29.4 %copy-start.5 = (bf16[768,256]{1,0:T(8,128)(2,1)S(1)}, bf16[768,256]{1,0:T(8,128)(2,1)}, u32[]{:S(2)}) copy-start(bf16[768,256]{1,0:T(8,128)(2,1)} %param.39) | copy-start | bytes 1179652
  187.9 11.8 %all-to-all-start.8 = ((bf16[16,16,768]{2,1,0:T(8,128)(2,1)}), bf16[16,16,768]{2,1,0:T(8,128)(2,1)S(1)}, u32[]{:S(2)}, u32[]{:S(2)}) async-start(bf16[16,16,768]{2,1,0:T(8,128)(2,1)} %broadcast_in_dim.11), calls=%async_computation.8 | async-start | bytes 786432 | tf_op jit(solution)/shard_map/all_to_all | solution.py:40
  200.7 16.9 %all-to-all-start.9 = ((bf16[16,16,256]{2,1,0:T(8,128)(2,1)}), bf16[16,16,256]{2,1,0:T(8,128)(2,1)S(1)}, u32[]{:S(2)}, u32[]{:S(2)}) async-start(bf16[16,16,256]{2,1,0:T(8,128)(2,1)} %bitcast.33), calls=%async_computation.9 | async-start | bytes 262144 | tf_op jit(solution)/shard_map/all_to_all | solution.py:18
Sparse Core Ops, SparseCore 0:
  120.5 32.4 all-gather.2
where the time goes:
time: 226 us; the launch traced here: 225 us
  blocking collectives  72.6 us (32%)
  waiting for transfers between devices  66.7 us (30%)
  starting transfers between devices  32.6 us (14%)
  local copies, waits for them, and re-layouts  17.5 us (8%)
  between operations  15 us (7%)
  matrix products  10.9 us (5%)
  other arithmetic  9.74 us (4%)
    all_to_all x3, blocking collectives, summed_on_arrival(): tiles = lax.all_to_all(in_blocks(array, dim, size), axis, 0, 0, tiled=True)  51.5 us
    all_gather x1, waiting for transfers between devices, total_of_pieces(): tiles = lax.all_gather(array, axis).astype(jnp.float32)  30.1 us
    all_to_all x3, waiting for transfers between devices, from_everyone(): return lax.all_to_all(copies, axis, split_axis=0, concat_axis=0, tiled=True)  24.6 us
    all_to_all x3, starting transfers between devices, from_everyone(): return lax.all_to_all(copies, axis, split_axis=0, concat_axis=0, tiled=True)  17.9 us
    all_to_all x1, blocking collectives, from_everyone(): return lax.all_to_all(copies, axis, split_axis=0, concat_axis=0, tiled=True)  12 us
    all_to_all x1, blocking collectives, body(): lax.all_to_all(stream_one.reshape(rows, 1, col_width), 'kv', split_axis=0...  9.06 us
    convert_element_type x3, local copies, waits for them, and re-layouts, body(): row_values = own_rows.astype(f32)  8.22 us
    all_to_all x1, starting transfers between devices, summed_on_arrival(): tiles = lax.all_to_all(in_blocks(array, dim, size), axis, 0, 0, tiled=True)  7.98 us
  transfers between devices with their start and end apart: 6, of which 6 were waited for; matrix products, arithmetic and copies ran while one was open for 3% of the time, Pallas kernels for 0%

commit v1 on v0

v1 whole, which is shorter than its diff:
```python
import jax
import jax.numpy as jnp
from jax import lax
from jax.experimental import pallas as pl
from jax.experimental.pallas import tpu as pltpu
from jax.sharding import PartitionSpec as P

EPS = 1e-06
MESH = pl.DeviceIdType.MESH
F32 = jnp.float32
BF16 = jnp.bfloat16
KV_OFFSETS = (
    (2, 2), (1, 2), (2, 1), (3, 2), (2, 3), (1, 1), (3, 3), (1, 3),
    (3, 1), (0, 2), (2, 0), (0, 1), (1, 0), (0, 3), (3, 0),
)
TP_OFFSETS = (
    (4, 0), (4, 1), (3, 0), (5, 0), (3, 1), (5, 1), (2, 0), (6, 0),
    (2, 1), (6, 1), (1, 0), (7, 0), (1, 1), (7, 1), (0, 1),
)


def nt(a, b):
    return lax.dot_general(a, b, (((1,), (1,)), ((), ())), preferred_element_type=F32)


def nn(a, b):
    return jnp.dot(a, b, preferred_element_type=F32)


def kernel(
    tok_hbm, mem_hbm, nrm_hbm, stab_hbm, g1_hbm, wg1_hbm, wu1_hbm, wd1_hbm, g2_hbm,
    wq_hbm, wk_hbm, wv_hbm, wi_hbm, wf_hbm, fb_hbm, wo_hbm, g3_hbm, wg3_hbm, wu3_hbm, wd3_hbm,
    res_ref, newmem_hbm, newnrm_ref, newstab_ref,
    mem, memb, memout, nrm, stab, g1, wg1, wu1, wd1, g2, wq, wk, wv, wif, fb, wo, g3, wg3, wu3, wd3,
    recv1, blk, send2, recv2, hid, recv3, send4, recv4, send5, recv5, cell, send6, recv6,
    send7, recv7, blk_t, send8, recv8, hid2, recv9, wd3t, send10, recv10,
    lsem, ssem, rsem, osem,
):
    kv = lax.axis_index("kv")
    tp = lax.axis_index("tp")
    y, x = kv // 4, kv % 4
    z, core = tp // 2, tp % 2
    kv_peers = [lax.rem(y + dy, 4) * 4 + lax.rem(x + dx, 4) for dy, dx in KV_OFFSETS]
    tp_peers = [lax.rem(z + dz, 8) * 2 + lax.rem(core + dc, 2) for dz, dc in TP_OFFSETS]
    diag = kv == tp

    pairs = [
        (tok_hbm, recv1.at[tp]), (wg1_hbm, wg1), (wu1_hbm, wu1), (g1_hbm, g1), (wd1_hbm, wd1),
        (wq_hbm, wq), (wk_hbm, wk), (wv_hbm, wv), (wi_hbm, wif.at[pl.ds(0, 16)]),
        (wf_hbm, wif.at[pl.ds(16, 16)]), (g2_hbm, g2), (mem_hbm, mem), (nrm_hbm, nrm),
        (stab_hbm, stab), (fb_hbm, fb), (wo_hbm, wo), (g3_hbm, g3), (wg3_hbm, wg3),
        (wu3_hbm, wu3), (wd3_hbm, wd3),
    ]
    loads = [pltpu.make_async_copy(s, d, lsem.at[i]) for i, (s, d) in enumerate(pairs)]
    for c in loads:
        c.start()
    (ld_tok, ld_wg1, ld_wu1, ld_g1, ld_wd1, ld_wq, ld_wk, ld_wv, ld_wi, ld_wf, ld_g2, ld_mem,
     ld_nrm, ld_stab, ld_fb, ld_wo, ld_g3, ld_wg3, ld_wu3, ld_wd3) = loads

    barrier = pltpu.get_barrier_semaphore()

    def greet(k, t):
        pl.semaphore_signal(barrier, inc=1, device_id=(k, t), device_id_type=MESH)

    for k in kv_peers:
        greet(k, tp)
    for t in tp_peers:
        greet(kv, t)

    @pl.loop(0, 16)
    def _(j):
        @pl.when(jnp.logical_not(jnp.logical_and(diag, j == tp)))
        def _():
            greet(tp, j)
            greet(j, kv)

    pl.semaphore_wait(barrier, jnp.where(diag, 60, 62))
    ld_tok.wait()

    def send(src, dst, phase, k, t):
        pltpu.make_async_remote_copy(
            src_ref=src, dst_ref=dst, send_sem=ssem.at[phase], recv_sem=rsem.at[phase],
            device_id=(k, t), device_id_type=MESH,
        ).start()

    def arrived(buf, phase, count=15):
        part = buf.at[pl.ds(0, count)]
        pltpu.make_async_copy(part, part, rsem.at[phase]).wait()

    def sent(buf, phase, count=15):
        part = buf.at[pl.ds(0, count)]
        pltpu.make_async_copy(part, part, ssem.at[phase]).wait()

    def gain_row(g, c):
        return jnp.concatenate([g[pl.ds(2 * c, 1), :], g[pl.ds(2 * c + 1, 1), :]], axis=1)

    for t in tp_peers:
        send(recv1.at[tp], recv1.at[tp], 0, kv, t)

    arrived(recv1, 0)
    blk[...] = recv1[...].reshape(256, 256).T

    def gate_up(block, gain, wg, wu, out, into, phase):
        vals = block.astype(F32)
        scaled = (vals * gain).astype(BF16)
        sq = jnp.sum(vals * vals, axis=1, keepdims=True)
        out[:, :, pl.ds(1536, 128)] = jnp.broadcast_to(sq, (256, 128)).astype(BF16).reshape(16, 16, 128)
        for n in range(3):
            cols = pl.ds(n * 256, 256)
            out[:, :, cols] = nn(scaled, wg[:, cols]).astype(BF16).reshape(16, 16, 256)
            out[:, :, pl.ds(768 + n * 256, 256)] = nn(scaled, wu[:, cols]).astype(BF16).reshape(16, 16, 256)
        for k in kv_peers:
            send(out.at[k], into.at[kv], phase, k, tp)
        into[pl.ds(kv, 1)] = out[pl.ds(kv, 1)]

    def hidden(into, phase, out, gathered, next_phase):
        arrived(into, phase)
        scale = lax.rsqrt(jnp.sum(into[:, :, pl.ds(1536, 128)].astype(F32), axis=0)[:, :1] / 4096 + EPS)
        gate = scale * jnp.sum(into[:, :, pl.ds(0, 768)].astype(F32), axis=0)
        up = scale * jnp.sum(into[:, :, pl.ds(768, 768)].astype(F32), axis=0)
        h = (gate / (1.0 + jnp.exp(-gate)) * up).astype(BF16)
        gathered[pl.ds(kv, 1)] = h[None]
        for k in kv_peers:
            send(gathered.at[kv], gathered.at[kv], next_phase, k, tp)

    def to_group(buf, into, phase):
        @pl.loop(0, 16)
        def _(j):
            @pl.when(jnp.logical_not(jnp.logical_and(diag, j == tp)))
            def _():
                send(buf, into.at[kv], phase, tp, j)

        @pl.when(diag)
        def _():
            into[pl.ds(kv, 1)] = buf[...][None]

    def from_group(buf, wait, phase):
        @pl.when(diag)
        def _():
            wait(buf, phase, 15)

        @pl.when(jnp.logical_not(diag))
        def _():
            wait(buf, phase, 16)

    ld_wg1.wait()
    ld_wu1.wait()
    ld_g1.wait()
    gate_up(blk[...], gain_row(g1, kv), wg1, wu1, send2, recv2, 1)
    ld_mem.wait()
    memb[...] = mem[...].astype(BF16)
    hidden(recv2, 1, hid, recv3, 2)
    ld_wd1.wait()
    arrived(recv3, 2)

    send4[...] = nn(recv3[...].reshape(256, 768), wd1[...]).astype(BF16).reshape(16, 16, 256)
    for t in tp_peers:
        send(send4.at[t], recv4.at[tp], 3, kv, t)
    recv4[pl.ds(tp, 1)] = send4[pl.ds(tp, 1)]
    for c in (ld_wq, ld_wk, ld_wv, ld_wi, ld_wf, ld_g2, ld_nrm, ld_stab, ld_fb):
        c.wait()
    arrived(recv4, 3)
    first = jnp.sum(recv4[...].astype(F32), axis=0)
    rows = pl.ds(pl.multiple_of(tp * 16, 16), 16)
    send5[...] = (blk[rows, :].astype(F32) + 0.5 * first).astype(BF16)

    to_group(send5, recv5, 4)
    from_group(recv5, arrived, 4)

    sq = jnp.zeros((16, 256), F32)
    for c in range(16):
        v = recv5[c].astype(F32)
        sq = sq + v * v
        cell[:, pl.ds(c * 256, 256)] = (v * gain_row(g2, c)).astype(BF16)
    scale = lax.rsqrt(jnp.sum(sq, axis=1, keepdims=True) / 4096 + EPS)
    query = scale * nn(cell[...], wq[...]) * 128 ** (-0.5)
    key = scale * nn(cell[...], wk[...])
    value = scale * nn(cell[...], wv[...])
    gates = nt(cell[...], wif[...])
    lane32 = lax.broadcasted_iota(jnp.int32, (16, 32), 1)
    input_pre = scale * jnp.sum(jnp.where(lane32 == tp, gates, 0.0), axis=1, keepdims=True)
    pre = scale * jnp.sum(jnp.where(lane32 == tp + 16, gates, 0.0), axis=1, keepdims=True) + fb[...]
    log_forget = jnp.minimum(pre, 0.0) - jnp.log1p(jnp.exp(-jnp.abs(pre)))
    eye = lax.broadcasted_iota(jnp.int32, (16, 16), 0) == lax.broadcasted_iota(jnp.int32, (16, 16), 1)
    old_stab = jnp.sum(jnp.where(eye, jnp.broadcast_to(stab[...], (16, 16)), 0.0), axis=1, keepdims=True)
    carried = log_forget + old_stab
    new_stab = jnp.maximum(carried, input_pre)
    keep = jnp.exp(carried - new_stab)
    admit = jnp.exp(input_pre - new_stab)
    match = jnp.sum(query * key, axis=1, keepdims=True)
    denom = keep * jnp.sum(nrm[...] * query, axis=1, keepdims=True) + admit * match
    qb = query.astype(BF16)
    row256 = lax.broadcasted_iota(jnp.int32, (16, 256), 0)
    recalled = jnp.zeros((16, 256), F32)
    for b in range(16):
        recalled = jnp.where(row256 == b, nt(qb, memb[b]), recalled)
    numer = keep * recalled + (admit * match) * value
    cell_out = (numer / jnp.maximum(jnp.abs(denom), 1.0)).astype(BF16)

    ld_wo.wait()
    for c in range(16):
        send6[c] = nn(cell_out, wo[:, pl.ds(c * 256, 256)]).astype(BF16)
    for t in tp_peers:
        send(send6.at[t], recv6.at[tp], 5, kv, t)
    recv6[pl.ds(tp, 1)] = send6[pl.ds(tp, 1)]

    newnrm_ref[...] = keep * nrm[...] + admit * key
    newstab_ref[...] = jnp.sum(jnp.where(eye, jnp.broadcast_to(new_stab, (16, 16)), 0.0), axis=0, keepdims=True)
    added = admit * key
    vh = value.astype(BF16)
    vl = (value - vh.astype(F32)).astype(BF16)
    vt = jnp.concatenate([vh.astype(F32), vl.astype(F32), vh.astype(F32)], axis=0).T.astype(BF16)
    row128 = lax.broadcasted_iota(jnp.int32, (16, 128), 0)
    kh = added.astype(BF16).astype(F32)
    kl = added - kh
    for b in range(16):
        khb = jnp.where(row128 == b, kh, 0.0)
        klb = jnp.where(row128 == b, kl, 0.0)
        outer = nn(vt, jnp.concatenate([khb, khb, klb], axis=0).astype(BF16))
        kb = jnp.sum(jnp.where(row128[:, :1] == b, keep, 0.0), axis=0, keepdims=True)
        memout[b] = kb * mem[b] + outer
    put = pltpu.make_async_copy(memout, newmem_hbm, osem)
    put.start()

    arrived(recv6, 5)
    mixed = jnp.sum(recv6[...].astype(F32), axis=0)
    send7[...] = (recv5[pl.ds(tp, 1)][0].astype(F32) + mixed).astype(BF16)

    to_group(send7, recv7, 6)
    for c in (ld_wg3, ld_wu3, ld_g3, ld_wd3):
        c.wait()
    wd3t[...] = wd3[...].T
    from_group(recv7, arrived, 6)

    block = recv7[...].reshape(256, 256)
    gate_up(block, gain_row(g3, kv), wg3, wu3, send8, recv8, 7)
    blk_t[...] = block.T
    hidden(recv8, 7, hid2, recv9, 8)
    arrived(recv9, 8)

    send10[...] = nt(wd3t[...], recv9[...].reshape(256, 768)).astype(BF16).reshape(16, 16, 256)
    for t in tp_peers:
        send(send10.at[t], recv10.at[tp], 9, kv, t)
    recv10[pl.ds(tp, 1)] = send10[pl.ds(tp, 1)]
    arrived(recv10, 9)
    last = jnp.sum(recv10[...].astype(F32), axis=0)
    res_ref[...] = (blk_t[rows, :].astype(F32) + 0.5 * last).astype(BF16)

    sent(recv1, 0)
    sent(send2, 1)
    sent(recv3, 2)
    sent(send4, 3)
    from_group(recv5, sent, 4)
    sent(send6, 5)
    from_group(recv7, sent, 6)
    sent(send8, 7)
    sent(recv9, 8)
    sent(send10, 9)
    put.wait()


def layer(
    tokens, memory, normalizer, stabilizer, first_gain, first_gate, first_up, first_down, mixer_gain,
    query_weight, key_weight, value_weight, input_weight, forget_weight, forget_bias, output_weight,
    last_gain, last_gate, last_up, last_down,
):
    any_ = pl.BlockSpec(memory_space=pl.ANY)
    vmem = pl.BlockSpec(memory_space=pltpu.VMEM)
    b = lambda *s: pltpu.VMEM(s, BF16)
    f = lambda *s: pltpu.VMEM(s, F32)
    scratch = [
        f(16, 256, 128), b(16, 256, 128), f(16, 256, 128), f(16, 128), f(1, 16),
        f(32, 128), b(256, 768), b(256, 768), b(768, 256), f(32, 128),
        b(4096, 128), b(4096, 128), b(4096, 256), b(32, 4096), f(1, 1), b(256, 4096),
        f(32, 128), b(256, 768), b(256, 768), b(768, 256),
        b(16, 16, 256), b(256, 256), b(16, 16, 1664), b(16, 16, 1664), b(16, 768), b(16, 16, 768),
        b(16, 16, 256), b(16, 16, 256), b(16, 256), b(16, 16, 256), b(16, 4096),
        b(16, 16, 256), b(16, 16, 256), b(16, 256), b(16, 16, 256), b(256, 256),
        b(16, 16, 1664), b(16, 16, 1664), b(16, 768), b(16, 16, 768), b(256, 768),
        b(16, 16, 256), b(16, 16, 256),
        pltpu.SemaphoreType.DMA((20,)), pltpu.SemaphoreType.DMA((10,)),
        pltpu.SemaphoreType.DMA((10,)), pltpu.SemaphoreType.DMA,
    ]
    res, new_mem, new_nrm, new_stab = pl.pallas_call(
        kernel,
        out_shape=(
            jax.ShapeDtypeStruct((16, 256), BF16),
            jax.ShapeDtypeStruct((16, 256, 128), F32),
            jax.ShapeDtypeStruct((16, 128), F32),
            jax.ShapeDtypeStruct((1, 16), F32),
        ),
        in_specs=[any_] * 20,
        out_specs=(vmem, any_, vmem, vmem),
        scratch_shapes=scratch,
        compiler_params=pltpu.CompilerParams(
            collective_id=0, has_side_effects=True, vmem_limit_bytes=60 * 1024 * 1024
        ),
        name="layer",
    )(
        tokens.T, memory.reshape(16, 256, 128), normalizer.reshape(16, 128), stabilizer.reshape(1, 16),
        first_gain.reshape(32, 128), first_gate, first_up, first_down, mixer_gain.reshape(32, 128),
        query_weight, key_weight, value_weight, input_weight.T, forget_weight.T,
        forget_bias.reshape(1, 1), output_weight, last_gain.reshape(32, 128), last_gate, last_up, last_down,
    )
    return res.T, new_mem.reshape(16, 1, 256, 128), new_nrm.reshape(16, 1, 128), new_stab.reshape(16, 1)


def solution(mesh):
    in_specs = (
        P(None, ("kv", "tp")), P("kv", "tp", None, None), P("kv", "tp", None), P("kv", "tp"), P(),
        P("kv", "tp"), P("kv", "tp"), P("tp", "kv"), P(), P(None, "tp"), P(None, "tp"), P(None, "tp"),
        P(), P(), P("tp"), P("tp", None), P(), P("kv", "tp"), P("kv", "tp"), P("tp", "kv"),
    )
    out_specs = (P(None, ("kv", "tp")), P("kv", "tp", None, None), P("kv", "tp", None), P("kv", "tp"))
    return jax.shard_map(layer, mesh=mesh, in_specs=in_specs, out_specs=out_specs, check_vma=False)
```

time: 226 us -> 97.8 us (0.43)
  Pallas kernels: 0 us -> 90.8 us
  blocking collectives: 72.6 us -> 0 us
  waiting for transfers between devices: 66.7 us -> 0 us
  starting transfers between devices: 32.6 us -> 0 us
  between operations: 15 us -> 1.3 us
  local copies, waits for them, and re-layouts: 17.5 us -> 5.54 us
  matrix products: 10.9 us -> 0 us
  other arithmetic: 9.74 us -> 0 us
    pallas_call x0 -> x1, Pallas kernels: none -> 90.8 us  [layer(): pl.pallas_call(kernel, out_shape=(jax.ShapeDtypeStruct((16, 256), BF16),...]
    all_to_all x5 -> x0, blocking collectives: 72.6 us -> none  [the longest x3 51.5 us: summed_on_arrival(): tiles = lax.all_to_all(in_blocks(array, dim, size), axis, 0, 0, tiled=True)]
    all_to_all x5 -> x0, waiting for transfers between devices: 36.5 us -> none  [the longest x3 24.6 us: from_everyone(): return lax.all_to_all(copies, axis, split_axis=0, concat_axis=0, tiled=True)]
    all_to_all x5 -> x0, starting transfers between devices: 32.4 us -> none  [the longest x3 17.9 us: from_everyone(): return lax.all_to_all(copies, axis, split_axis=0, concat_axis=0, tiled=True)]
    all_gather x1 -> x0, waiting for transfers between devices: 30.1 us -> none  [total_of_pieces(): tiles = lax.all_gather(array, axis).astype(jnp.float32)]
    dot_general x13 -> x0, matrix products: 10.9 us -> none  [the longest x1 1.83 us: body(): jnp.einsum('bhvd,bhd->bhv', memory, query, precision=lax.Precision.HIGHEST)]
    convert_element_type x6 -> x0, local copies, waits for them, and re-layouts: 9.36 us -> none  [the longest x3 8.22 us: body(): row_values = own_rows.astype(f32)]
    add x2 -> x0, other arithmetic: 3.74 us -> none  [the longest x1 2.91 us: body(): keep[..., None, None] * memory]
  transfers between devices with their start and end apart: 6 -> 0, of which waited for: 6 -> 0; matrix products, arithmetic and copies ran while one was open for 3% -> 0% of each run, Pallas kernels for 0% -> 0%
where the time goes in v1:
time: 97.8 us; the launch traced here: 97.6 us
  Pallas kernels  90.8 us (93%)
  local copies, waits for them, and re-layouts  5.54 us (6%)
  between operations  1.3 us (1%)
    pallas_call x1, Pallas kernels, layer(): pl.pallas_call(kernel, out_shape=(jax.ShapeDtypeStruct((16, 256), BF16),...  90.8 us
    unnamed x8, local copies, waits for them, and re-layouts  5.54 us

profile of v1, /device:TPU:1, one launch (start us, length us, event | category | flops | bytes accessed | tf_op | source)
XLA Modules:
  0.0 97.6 jit_solution(17002371365315543418)
XLA Ops:
  1.3 90.8 %layer.1 = (bf16[16,256]{1,0:T(8,128)(2,1)}, f32[16,256,128]{2,1,0:T(8,128)}, f32[16,128]{1,0:T(8,128)}, f32[1,16]{1,0:T(1,128)}) custom-call(bf16[16,256]{1,0:T(8,128)(2,1)} %bitcast.28, f32[16,256,128]{2,1,0:T(8,128)} %bitcast.20, f32[16,128]{1,0:T(8,128)} %bitcast.29, f32[1,16]{1,0:T(1,128)} %bitcast.30, f32[32,128]{1,0:T(8,128)} %bitcast.23, ...), custom_call_target="tpu_custom_call" | custom-call | tf_op jit(solution)/shard_map/layer/pallas_call | solution.py:284
  92.1 1.3 %copy.31 = bf16[256,16]{0,1:T(8,128)(2,1)} copy(bf16[256,16]{0,1:T(8,128)(2,1)} %bitcast.27) | data formatting | bytes 16384
  93.4 0.0 copy-start
  93.4 0.0 copy-start.1
  93.4 3.1 %copy.32 = f32[16,1,256,128]{3,2,1,0:T(8,128)} copy(f32[16,1,256,128]{3,2,1,0:T(8,128)} %bitcast.19) | data formatting | bytes 4194304
  96.5 0.0 copy-done
  96.5 0.6 copy.33
  97.1 0.0 copy-done.1
  97.1 0.5 copy.34
Async XLA Ops:
  93.4 3.1 %copy-start = (f32[16,128]{1,0:T(8,128)S(1)}, f32[16,128]{1,0:T(8,128)}, u32[]{:S(2)}) copy-start(f32[16,128]{1,0:T(8,128)} %get-tuple-element.10) | copy-start | bytes 24580
  93.4 3.7 %copy-start.1 = (f32[1,16]{1,0:T(1,128)S(1)}, f32[1,16]{1,0:T(1,128)}, u32[]{:S(2)}) copy-start(f32[1,16]{1,0:T(1,128)} %get-tuple-element.11) | copy-start | bytes 196

commit v2 on v1

v2 whole, which is shorter than its diff:
```python
import jax
import jax.numpy as jnp
from jax import lax
from jax.experimental import pallas as pl
from jax.experimental.pallas import tpu as pltpu
from jax.sharding import PartitionSpec as P

EPS = 1e-06
MESH = pl.DeviceIdType.MESH
F32 = jnp.float32
BF16 = jnp.bfloat16
KV_OFFSETS = (
    (2, 2), (1, 2), (2, 1), (3, 2), (2, 3), (1, 1), (3, 3), (1, 3),
    (3, 1), (0, 2), (2, 0), (0, 1), (1, 0), (0, 3), (3, 0),
)
TP_OFFSETS = (
    (4, 0), (4, 1), (3, 0), (5, 0), (3, 1), (5, 1), (2, 0), (6, 0),
    (2, 1), (6, 1), (1, 0), (7, 0), (1, 1), (7, 1), (0, 1),
)
WIDE = 1664


def nt(a, b):
    return lax.dot_general(a, b, (((1,), (1,)), ((), ())), preferred_element_type=F32)


def nn(a, b):
    return jnp.dot(a, b, preferred_element_type=F32)


def kernel(
    tok_hbm, mem_hbm, nrm_hbm, stab_hbm, g1_hbm, wg1_hbm, wu1_hbm, wd1_hbm, g2_hbm,
    wq_hbm, wk_hbm, wv_hbm, wi_hbm, wf_hbm, fb_hbm, wo_hbm, g3_hbm, wg3_hbm, wu3_hbm, wd3_hbm,
    res_ref, memout, newnrm_ref, newstab_ref,
    tok, mem, memb, nrm, stab, g1, wg1, wu1, wd1, g2, wq, wk, wv, wif, fb, wo, g3, wg3, wu3, wd3,
    recv1, blk, send2, recv2, send2b, recv2b, recv3, send4, recv4, send5, recv5, cell, send6, recv6,
    send7, recv7, blk_t, send8, recv8, send8b, recv8b, recv9, wd3t, send10, recv10,
    lsem, ssem, rsem,
):
    kv = lax.axis_index("kv")
    tp = lax.axis_index("tp")
    y, x = kv // 4, kv % 4
    z, core = tp // 2, tp % 2
    kv_peers = [lax.rem(y + dy, 4) * 4 + lax.rem(x + dx, 4) for dy, dx in KV_OFFSETS]
    tp_peers = [lax.rem(z + dz, 8) * 2 + lax.rem(core + dc, 2) for dz, dc in TP_OFFSETS]
    diag = kv == tp
    a_me = jnp.where(core == 0, x, y)
    b_me = jnp.where(core == 0, y, x)
    g_me = a_me * 4 + b_me
    a_peers = [lax.rem(a_me + d, 4) for d in (2, 1, 3)]
    b_peers = [lax.rem(b_me + d, 4) for d in (2, 1, 3)]

    def at(a, b):
        return jnp.where(core == 0, b * 4 + a, a * 4 + b)

    pairs = [
        (tok_hbm, tok), (wg1_hbm, wg1), (wu1_hbm, wu1), (g1_hbm, g1), (wd1_hbm, wd1),
        (wq_hbm, wq), (wk_hbm, wk), (wv_hbm, wv), (wi_hbm, wif.at[pl.ds(0, 16)]),
        (wf_hbm, wif.at[pl.ds(16, 16)]), (g2_hbm, g2), (mem_hbm, mem), (nrm_hbm, nrm),
        (stab_hbm, stab), (fb_hbm, fb), (wo_hbm, wo), (g3_hbm, g3), (wg3_hbm, wg3),
        (wu3_hbm, wu3), (wd3_hbm, wd3),
    ]
    loads = [pltpu.make_async_copy(s, d, lsem.at[i]) for i, (s, d) in enumerate(pairs)]
    for c in loads:
        c.start()
    (ld_tok, ld_wg1, ld_wu1, ld_g1, ld_wd1, ld_wq, ld_wk, ld_wv, ld_wi, ld_wf, ld_g2, ld_mem,
     ld_nrm, ld_stab, ld_fb, ld_wo, ld_g3, ld_wg3, ld_wu3, ld_wd3) = loads

    barrier = pltpu.get_barrier_semaphore()
    for k in kv_peers:
        pl.semaphore_signal(barrier, inc=1, device_id=(k, tp), device_id_type=MESH)
    for t in tp_peers:
        pl.semaphore_signal(barrier, inc=1, device_id=(kv, t), device_id_type=MESH)

    def send(src, dst, sem, k, t):
        pltpu.make_async_remote_copy(
            src_ref=src, dst_ref=dst, send_sem=ssem.at[sem], recv_sem=rsem.at[sem],
            device_id=(k, t), device_id_type=MESH,
        ).start()

    def arrived(buf, sem, count):
        part = buf.at[pl.ds(0, count)]
        pltpu.make_async_copy(part, part, rsem.at[sem]).wait()

    def sent(buf, sem, count):
        part = buf.at[pl.ds(0, count)]
        pltpu.make_async_copy(part, part, ssem.at[sem]).wait()

    def gain_row(g, c):
        return jnp.concatenate([g[pl.ds(2 * c, 1), :], g[pl.ds(2 * c + 1, 1), :]], axis=1)

    spot = lax.broadcasted_iota(jnp.int32, (256, 256), 1)
    seq = lax.broadcasted_iota(jnp.int32, (256, 256), 0)
    spot_row = ((spot % 128) // 8) * 16 + (spot // 128) * 8 + spot % 8
    order = jnp.where(seq == spot_row, 1.0, 0.0).astype(BF16)
    ld_tok.wait()
    ordered = nn(tok[...], order).astype(BF16)
    for h in range(2):
        recv1[h, pl.ds(tp, 1)] = ordered[:, h * 128 : h * 128 + 128][None]
    pl.semaphore_wait(barrier, 30)

    for h in range(2):
        for t in tp_peers:
            send(recv1.at[h, tp], recv1.at[h, tp], h, kv, t)

    def gate_up(h, block, gain, wg, wu, out, into, sem):
        vals = block.astype(F32)
        scaled = (vals * gain).astype(BF16)
        sq = jnp.sum(vals * vals, axis=1, keepdims=True)
        out[h, :, :, pl.ds(1536, 128)] = jnp.broadcast_to(sq, (128, 128)).astype(BF16).reshape(4, 32, 128)
        for n in range(3):
            cols = pl.ds(n * 256, 256)
            out[h, :, :, cols] = nn(scaled, wg[:, cols]).astype(BF16).reshape(4, 32, 256)
            out[h, :, :, pl.ds(768 + n * 256, 256)] = nn(scaled, wu[:, cols]).astype(BF16).reshape(4, 32, 256)
        for a in a_peers:
            send(out.at[h, a], into.at[h, a_me], sem, at(a, b_me), tp)
        into[h, pl.ds(a_me, 1)] = out[h, pl.ds(a_me, 1)]

    def second_sum(h, into, sem, out, next_into, next_sem):
        arrived(into.at[h], sem, 3)
        for n in range(0, WIDE, 128):
            cols = pl.ds(n, 128)
            total = jnp.sum(into[h, :, :, cols].astype(F32), axis=0)
            out[h, :, :, cols] = total.reshape(4, 8, 128).astype(BF16)
        for b in b_peers:
            send(out.at[h, b], next_into.at[h, b_me], next_sem, at(a_me, b), tp)
        next_into[h, pl.ds(b_me, 1)] = out[h, pl.ds(b_me, 1)]

    def hidden(h, into, sem, gathered, next_sem):
        arrived(into.at[h], sem, 3)
        total = jnp.sum(into[h].astype(F32), axis=0)
        scale = lax.rsqrt(total[:, 1536:1537] / 4096 + EPS)
        gate = scale * total[:, :768]
        up = scale * total[:, 768:1536]
        gathered[h, pl.ds(g_me, 1)] = (gate / (1.0 + jnp.exp(-gate)) * up).astype(BF16)[None]
        for k in kv_peers:
            send(gathered.at[h, g_me], gathered.at[h, g_me], next_sem, k, tp)

    def to_group(buf, into, sem):
        @pl.loop(0, 16)
        def _(j):
            @pl.when(jnp.logical_not(jnp.logical_and(diag, j == tp)))
            def _():
                send(buf, into.at[kv], sem, tp, j)

        @pl.when(diag)
        def _():
            into[pl.ds(kv, 1)] = buf[...][None]

    def from_group(buf, wait, sem):
        @pl.when(diag)
        def _():
            wait(buf, sem, 15)

        @pl.when(jnp.logical_not(diag))
        def _():
            wait(buf, sem, 16)

    gain = None
    for h in range(2):
        arrived(recv1.at[h], h, 15)
        block = recv1[h].reshape(256, 128).T
        blk[h] = block.reshape(16, 8, 256)
        if h == 0:
            ld_wg1.wait()
            ld_wu1.wait()
            ld_g1.wait()
            gain = gain_row(g1, kv)
        gate_up(h, block, gain, wg1, wu1, send2, recv2, 2 + h)
    for h in range(2):
        second_sum(h, recv2, 2 + h, send2b, recv2b, 4 + h)
    for h in range(2):
        hidden(h, recv2b, 4 + h, recv3, 6 + h)

    ld_wd1.wait()
    for h in range(2):
        arrived(recv3.at[h], 6 + h, 15)
        send4[h] = nn(recv3[h].reshape(128, 768), wd1[...]).astype(BF16).reshape(16, 8, 256)
        for t in tp_peers:
            send(send4.at[h, t], recv4.at[h, tp], 8 + h, kv, t)
        recv4[h, pl.ds(tp, 1)] = send4[h, pl.ds(tp, 1)]
    for c in (ld_wq, ld_wk, ld_wv, ld_wi, ld_wf, ld_g2, ld_nrm, ld_stab, ld_fb, ld_mem, ld_wo):
        c.wait()
    memb[...] = mem[...].astype(BF16)

    for h in range(2):
        arrived(recv4.at[h], 8 + h, 15)
        first = jnp.sum(recv4[h].astype(F32), axis=0)
        send5[h] = (blk[h, pl.ds(tp, 1)][0].astype(F32) + 0.5 * first).astype(BF16)
        to_group(send5.at[h], recv5.at[h], 10 + h)
    for h in range(2):
        from_group(recv5.at[h], arrived, 10 + h)

    sq = jnp.zeros((16, 256), F32)
    for c in range(16):
        v = jnp.concatenate([recv5[0, c].astype(F32), recv5[1, c].astype(F32)], axis=0)
        sq = sq + v * v
        cell[:, pl.ds(c * 256, 256)] = (v * gain_row(g2, c)).astype(BF16)
    scale = lax.rsqrt(jnp.sum(sq, axis=1, keepdims=True) / 4096 + EPS)
    query = scale * nn(cell[...], wq[...]) * 128 ** (-0.5)
    key = scale * nn(cell[...], wk[...])
    value = scale * nn(cell[...], wv[...])
    gates = nt(cell[...], wif[...])
    lane32 = lax.broadcasted_iota(jnp.int32, (16, 32), 1)
    input_pre = scale * jnp.sum(jnp.where(lane32 == tp, gates, 0.0), axis=1, keepdims=True)
    pre = scale * jnp.sum(jnp.where(lane32 == tp + 16, gates, 0.0), axis=1, keepdims=True) + fb[...]
    log_forget = jnp.minimum(pre, 0.0) - jnp.log1p(jnp.exp(-jnp.abs(pre)))
    eye = lax.broadcasted_iota(jnp.int32, (16, 16), 0) == lax.broadcasted_iota(jnp.int32, (16, 16), 1)
    old_stab = jnp.sum(jnp.where(eye, jnp.broadcast_to(stab[...], (16, 16)), 0.0), axis=1, keepdims=True)
    carried = log_forget + old_stab
    new_stab = jnp.maximum(carried, input_pre)
    keep = jnp.exp(carried - new_stab)
    admit = jnp.exp(input_pre - new_stab)
    match = jnp.sum(query * key, axis=1, keepdims=True)
    denom = keep * jnp.sum(nrm[...] * query, axis=1, keepdims=True) + admit * match
    qb = query.astype(BF16)
    row256 = lax.broadcasted_iota(jnp.int32, (16, 256), 0)
    recalled = jnp.zeros((16, 256), F32)
    for b in range(16):
        recalled = jnp.where(row256 == b, nt(qb, memb[b]), recalled)
    numer = keep * recalled + (admit * match) * value
    cell_out = (numer / jnp.maximum(jnp.abs(denom), 1.0)).astype(BF16)

    for c in range(16):
        send6[:, c] = nn(cell_out, wo[:, pl.ds(c * 256, 256)]).astype(BF16).reshape(2, 8, 256)
    for h in range(2):
        for t in tp_peers:
            send(send6.at[h, t], recv6.at[h, tp], 12 + h, kv, t)
        recv6[h, pl.ds(tp, 1)] = send6[h, pl.ds(tp, 1)]

    for c in (ld_wg3, ld_wu3, ld_g3, ld_wd3):
        c.wait()
    for h in range(2):
        arrived(recv6.at[h], 12 + h, 15)
        mixed = jnp.sum(recv6[h].astype(F32), axis=0)
        send7[h] = (recv5[h, pl.ds(tp, 1)][0].astype(F32) + mixed).astype(BF16)
        to_group(send7.at[h], recv7.at[h], 14 + h)

    wd3t[...] = wd3[...].T
    newnrm_ref[...] = keep * nrm[...] + admit * key
    newstab_ref[...] = jnp.sum(jnp.where(eye, jnp.broadcast_to(new_stab, (16, 16)), 0.0), axis=0, keepdims=True)
    added = admit * key
    vh = value.astype(BF16)
    vl = (value - vh.astype(F32)).astype(BF16)
    vt = jnp.concatenate([vh.astype(F32), vl.astype(F32), vh.astype(F32)], axis=0).T.astype(BF16)
    row128 = lax.broadcasted_iota(jnp.int32, (16, 128), 0)
    kh = added.astype(BF16).astype(F32)
    kl = added - kh
    for b in range(16):
        khb = jnp.where(row128 == b, kh, 0.0)
        klb = jnp.where(row128 == b, kl, 0.0)
        outer = nn(vt, jnp.concatenate([khb, khb, klb], axis=0).astype(BF16))
        kb = jnp.sum(jnp.where(row128[:, :1] == b, keep, 0.0), axis=0, keepdims=True)
        memout[b] = kb * mem[b] + outer

    gain = gain_row(g3, kv)
    for h in range(2):
        from_group(recv7.at[h], arrived, 14 + h)
        gate_up(h, recv7[h].reshape(128, 256), gain, wg3, wu3, send8, recv8, 16 + h)
    for h in range(2):
        blk_t[h] = recv7[h].reshape(128, 256).T
    for h in range(2):
        second_sum(h, recv8, 16 + h, send8b, recv8b, 18 + h)
    for h in range(2):
        hidden(h, recv8b, 18 + h, recv9, 20 + h)

    for h in range(2):
        arrived(recv9.at[h], 20 + h, 15)
        send10[h] = nt(wd3t[...], recv9[h].reshape(128, 768)).astype(BF16).reshape(16, 16, 128)
        for t in tp_peers:
            send(send10.at[h, t], recv10.at[h, tp], 22 + h, kv, t)
        recv10[h, pl.ds(tp, 1)] = send10[h, pl.ds(tp, 1)]
    halves = []
    rows = pl.ds(pl.multiple_of(tp * 16, 16), 16)
    for h in range(2):
        arrived(recv10.at[h], 22 + h, 15)
        last = jnp.sum(recv10[h].astype(F32), axis=0)
        halves.append((blk_t[h, rows, :].astype(F32) + 0.5 * last).astype(BF16))
    res_ref[...] = nt(jnp.concatenate(halves, axis=1), order).astype(BF16)

    for h in range(2):
        sent(recv1.at[h], h, 15)
        sent(send2.at[h], 2 + h, 3)
        sent(send2b.at[h], 4 + h, 3)
        sent(recv3.at[h], 6 + h, 15)
        sent(send4.at[h], 8 + h, 15)
        from_group(recv5.at[h], sent, 10 + h)
        sent(send6.at[h], 12 + h, 15)
        from_group(recv7.at[h], sent, 14 + h)
        sent(send8.at[h], 16 + h, 3)
        sent(send8b.at[h], 18 + h, 3)
        sent(recv9.at[h], 20 + h, 15)
        sent(send10.at[h], 22 + h, 15)


def finish(res, mem, nrm, stab, res_out, mem_out, nrm_out, stab_out, sem):
    pairs = ((mem, mem_out), (res, res_out), (nrm, nrm_out), (stab, stab_out))
    copies = [pltpu.make_async_copy(s, d, sem.at[i]) for i, (s, d) in enumerate(pairs)]
    for c in copies:
        c.start()
    for c in copies:
        c.wait()


def layer(
    tokens, memory, normalizer, stabilizer, first_gain, first_gate, first_up, first_down, mixer_gain,
    query_weight, key_weight, value_weight, input_weight, forget_weight, forget_bias, output_weight,
    last_gain, last_gate, last_up, last_down,
):
    hbm = pl.BlockSpec(memory_space=pltpu.HBM)
    vmem = pl.BlockSpec(memory_space=pltpu.VMEM)
    b = lambda *s: pltpu.VMEM(s, BF16)
    f = lambda *s: pltpu.VMEM(s, F32)
    wide = lambda *s: b(2, 4, *s, WIDE)
    small = lambda: b(2, 16, 8, 256)
    scratch = [
        b(16, 256), f(16, 256, 128), b(16, 256, 128), f(16, 128), f(1, 16),
        f(32, 128), b(256, 768), b(256, 768), b(768, 256), f(32, 128),
        b(4096, 128), b(4096, 128), b(4096, 256), b(32, 4096), f(1, 1), b(256, 4096),
        f(32, 128), b(256, 768), b(256, 768), b(768, 256),
        b(2, 16, 16, 128), small(), wide(32), wide(32), wide(8), wide(8), b(2, 16, 8, 768),
        small(), small(), b(2, 8, 256), small(), b(16, 4096),
        small(), small(), b(2, 8, 256), small(), b(2, 256, 128),
        wide(32), wide(32), wide(8), wide(8), b(2, 16, 8, 768), b(256, 768),
        b(2, 16, 16, 128), b(2, 16, 16, 128),
        pltpu.SemaphoreType.DMA((20,)), pltpu.SemaphoreType.DMA((24,)), pltpu.SemaphoreType.DMA((24,)),
    ]
    shapes = (((16, 256), BF16), ((16, 256, 128), F32), ((16, 128), F32), ((1, 16), F32))
    parts = pl.pallas_call(
        kernel,
        out_shape=tuple(pltpu.VMEM(*s) for s in shapes),
        in_specs=[hbm] * 20,
        out_specs=(vmem,) * 4,
        scratch_shapes=scratch,
        compiler_params=pltpu.CompilerParams(
            collective_id=0, has_side_effects=True, vmem_limit_bytes=64_900_000
        ),
        name="layer",
    )(*(v for v in (
        tokens.T, memory.reshape(16, 256, 128), normalizer.reshape(16, 128), stabilizer.reshape(1, 16),
        first_gain.reshape(32, 128), first_gate, first_up, first_down, mixer_gain.reshape(32, 128),
        query_weight, key_weight, value_weight, input_weight.T, forget_weight.T,
        forget_bias.reshape(1, 1), output_weight, last_gain.reshape(32, 128), last_gate, last_up, last_down,
    )))
    res, new_mem, new_nrm, new_stab = pl.pallas_call(
        finish,
        out_shape=tuple(jax.ShapeDtypeStruct(*s) for s in shapes),
        in_specs=[vmem] * 4,
        out_specs=(hbm,) * 4,
        scratch_shapes=[pltpu.SemaphoreType.DMA((4,))],
        compiler_params=pltpu.CompilerParams(vmem_limit_bytes=1024 * 1024),
        name="finish",
    )(*(pltpu.with_memory_space_constraint(v, pltpu.VMEM) for v in parts))
    return res.T, new_mem.reshape(16, 1, 256, 128), new_nrm.reshape(16, 1, 128), new_stab.reshape(16, 1)


def solution(mesh):
    in_specs = (
        P(None, ("kv", "tp")), P("kv", "tp", None, None), P("kv", "tp", None), P("kv", "tp"), P(),
        P("kv", "tp"), P("kv", "tp"), P("tp", "kv"), P(), P(None, "tp"), P(None, "tp"), P(None, "tp"),
        P(), P(), P("tp"), P("tp", None), P(), P("kv", "tp"), P("kv", "tp"), P("tp", "kv"),
    )
    out_specs = (P(None, ("kv", "tp")), P("kv", "tp", None, None), P("kv", "tp", None), P("kv", "tp"))
    return jax.shard_map(layer, mesh=mesh, in_specs=in_specs, out_specs=out_specs, check_vma=False)
```

time: 97.8 us -> 87.6 us (0.90)
  local copies, waits for them, and re-layouts: 5.54 us -> 0 us
  Pallas kernels: 90.8 us -> 86.2 us
    unnamed x8 -> x0, local copies, waits for them, and re-layouts: 5.54 us -> none
    pallas_call x1 -> x2, Pallas kernels: 90.8 us -> 86.2 us  [the longest x1 84.8 us: layer(): pl.pallas_call(kernel, out_shape=tuple((pltpu.VMEM(*s) for s in shapes)),...]
where the time goes in v2:
time: 87.6 us; the launch traced here: 87.4 us
  Pallas kernels  86.2 us (98%)
  between operations  1.29 us (1%)
    pallas_call x1, Pallas kernels, layer(): pl.pallas_call(kernel, out_shape=tuple((pltpu.VMEM(*s) for s in shapes)),...  84.8 us

profile of v2, /device:TPU:1, one launch (start us, length us, event | category | flops | bytes accessed | tf_op | source)
XLA Modules:
  0.0 87.4 jit_solution(12546235866145206275)
XLA Ops:
  1.3 84.8 %layer.1 = (bf16[16,256]{1,0:T(8,128)(2,1)S(1)}, f32[16,256,128]{2,1,0:T(8,128)S(1)}, f32[16,128]{1,0:T(8,128)S(1)}, f32[1,16]{1,0:T(1,128)S(1)}) custom-call(bf16[16,256]{1,0:T(8,128)(2,1)} %bitcast.25, f32[16,256,128]{2,1,0:T(8,128)} %bitcast.19, f32[16,128]{1,0:T(8,128)} %bitcast.26, f32[1,16]{1,0:T(1,128)} %bitcast.27, f32[32,128]{1,0:T(8,128)} %bitcast.22, ...), custom_call_target="tpu_custom_call" | custom-call | tf_op jit(solution)/shard_map/layer/pallas_call | solution.py:329
  86.1 1.4 %finish.1 = (bf16[16,256]{1,0:T(8,128)(2,1)}, f32[16,256,128]{2,1,0:T(8,128)}, f32[16,128]{1,0:T(8,128)}, f32[1,16]{1,0:T(1,128)}) custom-call(bf16[16,256]{1,0:T(8,128)(2,1)S(1)} %get-tuple-element.12.res, f32[16,256,128]{2,1,0:T(8,128)S(1)} %get-tuple-element.13.mem, f32[16,128]{1,0:T(8,128)S(1)} %get-tuple-element.14.nrm, f32[1,16]{1,0:T(1,128)S(1)} %get-tuple-element.15.stab), custom_call_target="tpu_custom_call" | custom-call | tf_op jit(solution)/shard_map/finish/pallas_call | solution.py:345

commit v3 on v2

--- a/solution.py
+++ b/solution.py
@@ -137,11 +137,12 @@
             send(gathered.at[h, g_me], gathered.at[h, g_me], next_sem, k, tp)
 
     def to_group(buf, into, sem):
-        @pl.loop(0, 16)
-        def _(j):
-            @pl.when(jnp.logical_not(jnp.logical_and(diag, j == tp)))
-            def _():
-                send(buf, into.at[kv], sem, tp, j)
+        for t in tp_peers:
+            send(buf, into.at[kv], sem, tp, t)
+
+        @pl.when(jnp.logical_not(diag))
+        def _():
+            send(buf, into.at[kv], sem, tp, tp)
 
         @pl.when(diag)
         def _():

time: 87.6 us -> 86.3 us (0.985)
  Pallas kernels: 86.2 us -> 84.8 us
    pallas_call x1, Pallas kernels: 84.8 us -> 83.5 us  [layer(): pl.pallas_call(kernel, out_shape=tuple((pltpu.VMEM(*s) for s in shapes)),...]
where the time goes in v3:
time: 86.3 us; the launch traced here: 86.1 us
  Pallas kernels  84.8 us (98%)
  between operations  1.29 us (1%)
    pallas_call x1, Pallas kernels, layer(): pl.pallas_call(kernel, out_shape=tuple((pltpu.VMEM(*s) for s in shapes)),...  83.5 us

profile of v3, /device:TPU:1, one launch (start us, length us, event | category | flops | bytes accessed | tf_op | source)
XLA Modules:
  0.0 86.1 jit_solution(13261623644383063860)
XLA Ops:
  1.3 83.5 %layer.1 = (bf16[16,256]{1,0:T(8,128)(2,1)S(1)}, f32[16,256,128]{2,1,0:T(8,128)S(1)}, f32[16,128]{1,0:T(8,128)S(1)}, f32[1,16]{1,0:T(1,128)S(1)}) custom-call(bf16[16,256]{1,0:T(8,128)(2,1)} %bitcast.25, f32[16,256,128]{2,1,0:T(8,128)} %bitcast.19, f32[16,128]{1,0:T(8,128)} %bitcast.26, f32[1,16]{1,0:T(1,128)} %bitcast.27, f32[32,128]{1,0:T(8,128)} %bitcast.22, ...), custom_call_target="tpu_custom_call" | custom-call | tf_op jit(solution)/shard_map/layer/pallas_call | solution.py:330
  84.8 1.4 %finish.1 = (bf16[16,256]{1,0:T(8,128)(2,1)}, f32[16,256,128]{2,1,0:T(8,128)}, f32[16,128]{1,0:T(8,128)}, f32[1,16]{1,0:T(1,128)}) custom-call(bf16[16,256]{1,0:T(8,128)(2,1)S(1)} %get-tuple-element.12.res, f32[16,256,128]{2,1,0:T(8,128)S(1)} %get-tuple-element.13.mem, f32[16,128]{1,0:T(8,128)S(1)} %get-tuple-element.14.nrm, f32[1,16]{1,0:T(1,128)S(1)} %get-tuple-element.15.stab), custom_call_target="tpu_custom_call" | custom-call | tf_op jit(solution)/shard_map/finish/pallas_call | solution.py:346

commit v4 on v3

--- a/solution.py
+++ b/solution.py
@@ -44,14 +44,14 @@
     kv_peers = [lax.rem(y + dy, 4) * 4 + lax.rem(x + dx, 4) for dy, dx in KV_OFFSETS]
     tp_peers = [lax.rem(z + dz, 8) * 2 + lax.rem(core + dc, 2) for dz, dc in TP_OFFSETS]
     diag = kv == tp
-    a_me = jnp.where(core == 0, x, y)
-    b_me = jnp.where(core == 0, y, x)
+    a_me = jnp.where(core == 1, x, y)
+    b_me = jnp.where(core == 1, y, x)
     g_me = a_me * 4 + b_me
-    a_peers = [lax.rem(a_me + d, 4) for d in (2, 1, 3)]
-    b_peers = [lax.rem(b_me + d, 4) for d in (2, 1, 3)]
+    a_peers = [lax.rem(a_me + d, 4) for d in (2, 3, 1)]
+    b_peers = [lax.rem(b_me + d, 4) for d in (2, 3, 1)]
 
     def at(a, b):
-        return jnp.where(core == 0, b * 4 + a, a * 4 + b)
+        return jnp.where(core == 1, b * 4 + a, a * 4 + b)
 
     pairs = [
         (tok_hbm, tok), (wg1_hbm, wg1), (wu1_hbm, wu1), (g1_hbm, g1), (wd1_hbm, wd1),

time: 86.3 us -> 83 us (0.962)
  Pallas kernels: 84.8 us -> 81.6 us
    pallas_call x1, Pallas kernels: 83.5 us -> 80.2 us  [layer(): pl.pallas_call(kernel, out_shape=tuple((pltpu.VMEM(*s) for s in shapes)),...]
where the time goes in v4:
time: 83 us; the launch traced here: 82.9 us
  Pallas kernels  81.6 us (98%)
  between operations  1.29 us (2%)
    pallas_call x1, Pallas kernels, layer(): pl.pallas_call(kernel, out_shape=tuple((pltpu.VMEM(*s) for s in shapes)),...  80.2 us

profile of v4, /device:TPU:1, one launch (start us, length us, event | category | flops | bytes accessed | tf_op | source)
XLA Modules:
  0.0 82.9 jit_solution(12450368825527336437)
XLA Ops:
  1.3 80.2 %layer.1 = (bf16[16,256]{1,0:T(8,128)(2,1)S(1)}, f32[16,256,128]{2,1,0:T(8,128)S(1)}, f32[16,128]{1,0:T(8,128)S(1)}, f32[1,16]{1,0:T(1,128)S(1)}) custom-call(bf16[16,256]{1,0:T(8,128)(2,1)} %bitcast.25, f32[16,256,128]{2,1,0:T(8,128)} %bitcast.19, f32[16,128]{1,0:T(8,128)} %bitcast.26, f32[1,16]{1,0:T(1,128)} %bitcast.27, f32[32,128]{1,0:T(8,128)} %bitcast.22, ...), custom_call_target="tpu_custom_call" | custom-call | tf_op jit(solution)/shard_map/layer/pallas_call | solution.py:330
  81.5 1.4 %finish.1 = (bf16[16,256]{1,0:T(8,128)(2,1)}, f32[16,256,128]{2,1,0:T(8,128)}, f32[16,128]{1,0:T(8,128)}, f32[1,16]{1,0:T(1,128)}) custom-call(bf16[16,256]{1,0:T(8,128)(2,1)S(1)} %get-tuple-element.12.res, f32[16,256,128]{2,1,0:T(8,128)S(1)} %get-tuple-element.13.mem, f32[16,128]{1,0:T(8,128)S(1)} %get-tuple-element.14.nrm, f32[1,16]{1,0:T(1,128)S(1)} %get-tuple-element.15.stab), custom_call_target="tpu_custom_call" | custom-call | tf_op jit(solution)/shard_map/finish/pallas_call | solution.py:346

commit v5 on v4

--- a/solution.py
+++ b/solution.py
@@ -53,6 +53,12 @@
     def at(a, b):
         return jnp.where(core == 1, b * 4 + a, a * 4 + b)
 
+    barrier = pltpu.get_barrier_semaphore()
+    for t in tp_peers:
+        pl.semaphore_signal(barrier, inc=1, device_id=(kv, t), device_id_type=MESH)
+    for k in kv_peers:
+        pl.semaphore_signal(barrier, inc=1, device_id=(k, tp), device_id_type=MESH)
+
     pairs = [
         (tok_hbm, tok), (wg1_hbm, wg1), (wu1_hbm, wu1), (g1_hbm, g1), (wd1_hbm, wd1),
         (wq_hbm, wq), (wk_hbm, wk), (wv_hbm, wv), (wi_hbm, wif.at[pl.ds(0, 16)]),
@@ -65,12 +71,6 @@
         c.start()
     (ld_tok, ld_wg1, ld_wu1, ld_g1, ld_wd1, ld_wq, ld_wk, ld_wv, ld_wi, ld_wf, ld_g2, ld_mem,
      ld_nrm, ld_stab, ld_fb, ld_wo, ld_g3, ld_wg3, ld_wu3, ld_wd3) = loads
-
-    barrier = pltpu.get_barrier_semaphore()
-    for k in kv_peers:
-        pl.semaphore_signal(barrier, inc=1, device_id=(k, tp), device_id_type=MESH)
-    for t in tp_peers:
-        pl.semaphore_signal(barrier, inc=1, device_id=(kv, t), device_id_type=MESH)
 
     def send(src, dst, sem, k, t):
         pltpu.make_async_remote_copy(
@@ -237,6 +237,12 @@
         send7[h] = (recv5[h, pl.ds(tp, 1)][0].astype(F32) + mixed).astype(BF16)
         to_group(send7.at[h], recv7.at[h], 14 + h)
 
+    gain = gain_row(g3, kv)
+    for h in range(2):
+        from_group(recv7.at[h], arrived, 14 + h)
+        gate_up(h, recv7[h].reshape(128, 256), gain, wg3, wu3, send8, recv8, 16 + h)
+    for h in range(2):
+        blk_t[h] = recv7[h].reshape(128, 256).T
     wd3t[...] = wd3[...].T
     newnrm_ref[...] = keep * nrm[...] + admit * key
     newstab_ref[...] = jnp.sum(jnp.where(eye, jnp.broadcast_to(new_stab, (16, 16)), 0.0), axis=0, keepdims=True)
@@ -254,12 +260,6 @@
         kb = jnp.sum(jnp.where(row128[:, :1] == b, keep, 0.0), axis=0, keepdims=True)
         memout[b] = kb * mem[b] + outer
 
-    gain = gain_row(g3, kv)
-    for h in range(2):
-        from_group(recv7.at[h], arrived, 14 + h)
-        gate_up(h, recv7[h].reshape(128, 256), gain, wg3, wu3, send8, recv8, 16 + h)
-    for h in range(2):
-        blk_t[h] = recv7[h].reshape(128, 256).T
     for h in range(2):
         second_sum(h, recv8, 16 + h, send8b, recv8b, 18 + h)
     for h in range(2):

time: 83 us -> 83 us (level)
  no operation moved by 1% of the time
where the time goes in v5:
time: 83 us; the launch traced here: 82.9 us
  Pallas kernels  81.6 us (98%)
  between operations  1.29 us (2%)
    pallas_call x1, Pallas kernels, layer(): pl.pallas_call(kernel, out_shape=tuple((pltpu.VMEM(*s) for s in shapes)),...  80.2 us

profile of v5, /device:TPU:1, one launch (start us, length us, event | category | flops | bytes accessed | tf_op | source)
XLA Modules:
  0.0 82.9 jit_solution(10306375632638747140)
XLA Ops:
  1.3 80.2 %layer.1 = (bf16[16,256]{1,0:T(8,128)(2,1)S(1)}, f32[16,256,128]{2,1,0:T(8,128)S(1)}, f32[16,128]{1,0:T(8,128)S(1)}, f32[1,16]{1,0:T(1,128)S(1)}) custom-call(bf16[16,256]{1,0:T(8,128)(2,1)} %bitcast.25, f32[16,256,128]{2,1,0:T(8,128)} %bitcast.19, f32[16,128]{1,0:T(8,128)} %bitcast.26, f32[1,16]{1,0:T(1,128)} %bitcast.27, f32[32,128]{1,0:T(8,128)} %bitcast.22, ...), custom_call_target="tpu_custom_call" | custom-call | tf_op jit(solution)/shard_map/layer/pallas_call | solution.py:330
  81.5 1.4 %finish.1 = (bf16[16,256]{1,0:T(8,128)(2,1)}, f32[16,256,128]{2,1,0:T(8,128)}, f32[16,128]{1,0:T(8,128)}, f32[1,16]{1,0:T(1,128)}) custom-call(bf16[16,256]{1,0:T(8,128)(2,1)S(1)} %get-tuple-element.12.res, f32[16,256,128]{2,1,0:T(8,128)S(1)} %get-tuple-element.13.mem, f32[16,128]{1,0:T(8,128)S(1)} %get-tuple-element.14.nrm, f32[1,16]{1,0:T(1,128)S(1)} %get-tuple-element.15.stab), custom_call_target="tpu_custom_call" | custom-call | tf_op jit(solution)/shard_map/finish/pallas_call | solution.py:346
